TPU v7x, 32 devices: a whole 2x2x4 slice. The times are simulated.
32 devices in a mesh: sp: 16 (over z, y, core), tp: 2 (over x).
Axes of the slice: x: 2, y: 2, z: 4, core: 2. Of those that a mesh axis runs over, the one named last changes fastest.
Arguments:
- queries: bfloat16 [16384, 1024], P('sp', 'tp'), may hold values from -8 to 8
- keyvals: bfloat16 [16384, 8, 128], P('sp', 'tp'), may hold values from -8 to 8
- head_sink_logit: float32 [16], P('tp'), may hold values from 2 to 7
- doc_ids: int32 [16384], P('sp'), may hold values from 0 to 7, never falling along the last dimension, each value on 1 to 4096 neighbouring positions
- stream_in: bfloat16 [16384, 2048], P(('sp', 'tp')), may hold values from -6 to 6
- out_weight: bfloat16 [1024, 2048], replicated, may hold values from -1.5 to 1.5
- first_gain: float32 [2048], replicated, may hold values from 0.1 to 1.9
- up_weight: bfloat16 [2048, 8192], P('sp', 'tp'), may hold values from -0.125 to 0.125
- down_weight: bfloat16 [8192, 2048], P('tp', 'sp'), may hold values from -0.0625 to 0.0625
- second_gain: float32 [2048], replicated, may hold values from 0.1 to 1.9
Outputs:
- layer_out: bfloat16 [16384, 2048], P(('sp', 'tp'))
Inputs may be any that keep to these rules, and one draw needn't show every extreme that they name: `doc_ids`: document numbers never fall along the sequence.
All inputs are finite; a program needn't handle non-finite values.
Results may differ from a plain program's by a relative error of at most 0.013.
Values may be sent and summed in bfloat16 or wider, within the bound.
A program may use at most 128 MiB of HBM per device.

v0:
```python
import jax
import jax.numpy as jnp
from jax import lax
from jax.sharding import PartitionSpec as P

HEAD_SIZE = 64
WINDOW_REACH = 128
NEG_LARGE = -1e30
NORM_EPS = 1e-05


def padded(block, sides, width):
    for axis, dim in sides:
        count = lax.axis_size(axis)
        forward = [(i, i + 1) for i in range(count - 1)]
        backward = [(target, source) for source, target in forward]
        low = lax.ppermute(
            lax.slice_in_dim(block, block.shape[dim] - width, None, axis=dim), axis, forward
        )
        high = lax.ppermute(lax.slice_in_dim(block, 0, width, axis=dim), axis, backward)
        block = jnp.concatenate([low, block, high], axis=dim)
    return block


def layer_norm(stream, gain_row):
    centre = jnp.mean(stream, axis=-1, keepdims=True)
    shifted = stream - centre
    spread = jnp.mean(shifted * shifted, axis=-1, keepdims=True)
    return shifted * lax.rsqrt(spread + NORM_EPS) * gain_row


def attend(queries, keyvals, head_sink_logit, doc_ids):
    tok_rows = queries.shape[0]
    kv_heads = keyvals.shape[1]
    heads_per_group = queries.shape[1] // (HEAD_SIZE * kv_heads)
    block_list = tok_rows // WINDOW_REACH
    score_scale = HEAD_SIZE ** (-0.5)
    doc_marks = doc_ids.astype(jnp.bfloat16)
    rim_keys, rim_docs = (
        padded(keyvals, (("sp", 0),), WINDOW_REACH),
        padded(doc_marks, (("sp", 0),), WINDOW_REACH),
    )
    padded_rows = rim_keys.reshape(block_list + 2, WINDOW_REACH, kv_heads, 2 * HEAD_SIZE)
    banded = jnp.concatenate([padded_rows[:-2], padded_rows[1:-1], padded_rows[2:]], axis=1)
    doc_ext = rim_docs.reshape(block_list + 2, WINDOW_REACH)
    doc_band = jnp.concatenate([doc_ext[:-2], doc_ext[1:-1], doc_ext[2:]], axis=1)
    offset = lax.axis_index("sp") * tok_rows
    total_rows = tok_rows * lax.axis_size("sp")
    query_pos = offset + jnp.arange(tok_rows, dtype=jnp.int32).reshape(block_list, WINDOW_REACH, 1)
    key_pos = (
        offset
        + (
            jnp.arange(block_list, dtype=jnp.int32)[:, None] * WINDOW_REACH
            + jnp.arange(3 * WINDOW_REACH, dtype=jnp.int32)[None, :]
            - WINDOW_REACH
        )[:, None, :]
    )
    allowed = (
        (jnp.abs(query_pos - key_pos) <= WINDOW_REACH)
        & (key_pos >= 0)
        & (key_pos < total_rows)
        & (doc_marks.reshape(block_list, WINDOW_REACH, 1) == doc_band[:, None, :])
    )
    query_block_list = queries.reshape(
        block_list, WINDOW_REACH, kv_heads, heads_per_group, HEAD_SIZE
    )
    scores = (
        jnp.einsum(
            "nqhgd,nkhd->nhgqk",
            query_block_list,
            banded[..., :HEAD_SIZE],
            preferred_element_type=jnp.float32,
        )
        * score_scale
    )
    scores = jnp.where(allowed[:, None, None], scores, NEG_LARGE)
    sink_col = head_sink_logit.reshape(kv_heads, heads_per_group)[None, :, :, None, None]
    highest = jnp.maximum(jnp.max(scores, axis=-1, keepdims=True), sink_col)
    powers = jnp.exp(scores - highest)
    denominator = jnp.sum(powers, axis=-1, keepdims=True) + jnp.exp(sink_col - highest)
    weights = (powers / denominator).astype(jnp.bfloat16)
    mixed_out = jnp.einsum(
        "nhgqk,nkhd->nqhgd", weights, banded[..., HEAD_SIZE:], preferred_element_type=jnp.float32
    )
    return mixed_out.astype(jnp.bfloat16).reshape(tok_rows, kv_heads * heads_per_group * HEAD_SIZE)


def per_device(
    queries,
    keyvals,
    head_sink_logit,
    doc_ids,
    stream_in,
    out_weight,
    first_gain,
    up_weight,
    down_weight,
    second_gain,
):
    up_whole = lax.all_gather(up_weight, "sp", axis=0, tiled=True)
    down_whole = lax.all_gather(down_weight, "sp", axis=1, tiled=True)
    attended = attend(queries, keyvals, head_sink_logit, doc_ids)
    tp_count = lax.axis_size("tp")
    own_rows = attended.shape[0] // tp_count
    by_peer = attended.reshape(tp_count, own_rows, attended.shape[1])
    projected = jnp.dot(
        lax.all_to_all(by_peer, "tp", split_axis=0, concat_axis=2, tiled=True)[0],
        out_weight,
        preferred_element_type=jnp.float32,
    )[None][0]
    first_stream = layer_norm(stream_in.astype(jnp.float32) + projected, first_gain).astype(
        jnp.bfloat16
    )
    hidden = jnp.dot(
        lax.all_gather(first_stream, "tp", axis=0, tiled=True),
        up_whole,
        preferred_element_type=jnp.float32,
    )
    active = jnp.square(jnp.maximum(hidden, 0.0)).astype(jnp.bfloat16)
    mixed_out = lax.psum_scatter(
        jnp.dot(active, down_whole, preferred_element_type=jnp.float32).astype(jnp.bfloat16),
        "tp",
        scatter_dimension=0,
        tiled=True,
    ).astype(jnp.float32)
    return layer_norm(first_stream.astype(jnp.float32) + mixed_out, second_gain).astype(
        jnp.bfloat16
    )


def solution(mesh):
    return jax.shard_map(
        per_device,
        mesh=mesh,
        in_specs=(
            P("sp", "tp"),
            P("sp", "tp", None),
            P("tp"),
            P("sp"),
            P(("sp", "tp"), None),
            P(),
            P(),
            P("sp", "tp"),
            P("tp", "sp"),
            P(),
        ),
        out_specs=P(("sp", "tp"), None),
        check_vma=False,
    )
```

profile of v0, /device:TPU:0, one launch (start us, length us, event | category | flops | bytes accessed | tf_op | source)
XLA Modules:
  0.0 477.8 jit_solution(12057201046544516895)
XLA Ops:
  6.5 0.8 convert_element_type.34
  7.3 2.4 collective-permute-start.2
  9.7 1.3 collective-permute-start.3
  11.0 1.4 copy.26
  12.4 5.8 %collective-permute-start = (bf16[128,4,128]{2,0,1:T(8,128)(2,1)S(1)}, bf16[128,4,128]{2,0,1:T(8,128)(2,1)}, u32[]{:S(2)}, u32[]{:S(2)}) collective-permute-start(bf16[128,4,128]{2,0,1:T(8,128)(2,1)S(1)} %get-tuple-element.7), channel_id=1, source_target_pairs={{0,2},{2,4},{4,6},{6,8},{8,10},{10,12},{12,14},{14,16},{16,18},{18... | collective-permute-start | bytes 393224 | tf_op jit(solution)/shard_map/ppermute | solution.py:17
  18.2 1.3 collective-permute-start.1
  19.5 0.7 convert_bitcast_fusion
  20.4 2.3 copy.32
  22.6 2.1 reshape.167
  24.8 2.3 fusion.9
  27.1 1.3 pad_maximum_fusion.2
  29.7 1.8 pad_maximum_fusion
  31.6 2.5 fusion.1
  34.3 3.4 fusion
  37.8 3.6 fusion.11
  41.4 0.7 copy.37
  42.8 17.2 %all_to_all.15 = bf16[2,512,512]{1,2,0:T(8,128)(2,1)S(1)} all-to-all(bf16[2,512,512]{1,2,0:T(8,128)(2,1)S(1)} %copy.38), channel_id=1, replica_groups=mesh['sp'=16,'tp'=2] {'tp'}, dimensions={0} | all-to-all | bytes 2097152 | tf_op jit(solution)/shard_map/all_to_all | solution.py:107
  60.0 4.2 fusion.20
  64.8 1.4 copy-done
  66.1 1.9 multiply_convert_fusion.2
  68.1 0.7 all-gather.6.cloned.1.call-update
  68.9 0.7 all-gather.8.cloned.1.call-update
  69.6 56.9 %all-gather.4.cloned.1.call-done = bf16[1024,2048]{1,0:T(8,128)(2,1)} async-done(((bf16[512,2048]{1,0:T(8,128)(2,1)}), bf16[1024,2048]{1,0:T(8,128)(2,1)}) %all-gather.4.cloned.1.call-update) | async-done | bytes 4194320 | tf_op jit(solution)/shard_map/all_gather | solution.py:115
  126.5 128.6 %all-gather.6.cloned.1.call-done = bf16[2048,4096]{1,0:T(8,128)(2,1)} async-done(((bf16[128,4096]{1,0:T(8,128)(2,1)}), bf16[2048,4096]{1,0:T(8,128)(2,1)}) %all-gather.6.cloned.1.call-update) | async-done | bytes 16777232 | tf_op jit(solution)/shard_map/all_gather | solution.py:100
  255.1 22.9 %fusion.44 = bf16[1024,4096]{1,0:T(8,128)(2,1)} fusion(bf16[2048,4096]{1,0:T(8,128)(2,1)} %all-gather.6.cloned.1.call-done, bf16[1024,2048]{1,0:T(8,128)(2,1)} %all-gather.4.cloned.1.call-done), kind=kOutput, calls=%bitcast_fusion.1.clone.1 | convolution fusion | flops 17192452096 | bytes 29360128 | tf_op jit(solution)/shard_map/dot_general | solution.py:114
  278.0 107.4 %all-gather.8.cloned.1.call-done = bf16[4096,2048]{1,0:T(8,128)(2,1)} async-done(((bf16[4096,128]{1,0:T(8,128)(2,1)}), bf16[4096,2048]{1,0:T(8,128)(2,1)}) %all-gather.8.cloned.1.call-update) | async-done | bytes 16777232 | tf_op jit(solution)/shard_map/all_gather | solution.py:101
  385.4 23.7 %convolution_convert_fusion = bf16[1024,2048]{1,0:T(8,128)(2,1)} fusion(bf16[4096,2048]{1,0:T(8,128)(2,1)} %all-gather.8.cloned.1.call-done, bf16[1024,4096]{1,0:T(8,128)(2,1)} %fusion.44), kind=kOutput, calls=%fused_computation.15 | convolution fusion | flops 17181966336 | bytes 29360128 | tf_op jit(solution)/shard_map/dot_general | solution.py:121
  409.1 52.7 %reduce-scatter.2.cloned.1.call-done = bf16[512,2048]{1,0:T(8,128)(2,1)} async-done(((bf16[1024,2048]{1,0:T(8,128)(2,1)}), bf16[512,2048]{1,0:T(8,128)(2,1)}) %reduce-scatter.2.cloned.1.call-update) | async-done | bytes 2097168 | tf_op jit(solution)/shard_map/reduce_scatter | solution.py:120
  461.8 3.9 fusion.4
  465.8 0.7 copy-done.2
  466.5 1.2 multiply_reduce_fusion
  467.8 3.5 multiply_convert_fusion.1
  (50 shorter events, 3.3 us)
Async XLA Ops:
  6.5 16.1 %copy-start.7 = (bf16[1024,512]{1,0:T(8,128)(2,1)S(1)}, bf16[1024,512]{1,0:T(8,128)(2,1)}, u32[]{:S(2)}) copy-start(bf16[1024,512]{1,0:T(8,128)(2,1)} %param.10) | copy-start | bytes 3145732
  6.5 18.2 %copy-start.10 = (f32[8]{0:T(128)S(1)}, f32[8]{0:T(128)}, u32[]{:S(2)}) copy-start(f32[8]{0:T(128)} %param.12) | copy-start | bytes 100
  6.5 119.9 %all-gather.4.cloned.1.call-start = ((), (), s32[]{:S(2)}) async-start(), calls=%async_computation.2 | async-start | bytes 6291456 | tf_op jit(solution)/shard_map/all_gather | solution.py:115
  7.3 17.5 %collective-permute-start.2 = (bf16[128]{0:T(256)(128)(2,1)S(1)}, bf16[128]{0:T(256)(128)(2,1)S(1)}, u32[]{:S(2)}, u32[]{:S(2)}) collective-permute-start(bf16[128]{0:T(256)(128)(2,1)S(1)} %get-tuple-element.11), channel_id=1, source_target_pairs={{0,2},{2,4},{4,6},{6,8},{8,10},{10,12},{12,14},{14,16},{16,18},{18... | collective-permute-start | bytes 776 | tf_op jit(solution)/shard_map/ppermute | solution.py:17
  9.7 15.1 %collective-permute-start.3 = (bf16[128]{0:T(256)(128)(2,1)S(1)}, bf16[128]{0:T(256)(128)(2,1)S(1)}, u32[]{:S(2)}, u32[]{:S(2)}) collective-permute-start(bf16[128]{0:T(256)(128)(2,1)S(1)} %get-tuple-element.12), channel_id=1, source_target_pairs={{2,0},{4,2},{6,4},{8,6},{10,8},{12,10},{14,12},{16,14},{18,16},{20... | collective-permute-start | bytes 776 | tf_op jit(solution)/shard_map/ppermute | solution.py:20
  12.4 14.7 %collective-permute-start = (bf16[128,4,128]{2,0,1:T(8,128)(2,1)S(1)}, bf16[128,4,128]{2,0,1:T(8,128)(2,1)}, u32[]{:S(2)}, u32[]{:S(2)}) collective-permute-start(bf16[128,4,128]{2,0,1:T(8,128)(2,1)S(1)} %get-tuple-element.7), channel_id=1, source_target_pairs={{0,2},{2,4},{4,6},{6,8},{8,10},{10,12},{12,14},{14,16},{16,18},{18... | collective-permute-start | bytes 393224 | tf_op jit(solution)/shard_map/ppermute | solution.py:17
  18.2 8.9 %collective-permute-start.1 = (bf16[128,4,128]{2,0,1:T(8,128)(2,1)S(1)}, bf16[128,4,128]{2,0,1:T(8,128)(2,1)}, u32[]{:S(2)}, u32[]{:S(2)}) collective-permute-start(bf16[128,4,128]{2,0,1:T(8,128)(2,1)S(1)} %get-tuple-element.8), channel_id=1, source_target_pairs={{2,0},{4,2},{6,4},{8,6},{10,8},{12,10},{14,12},{16,14},{18,16},{20... | collective-permute-start | bytes 393224 | tf_op jit(solution)/shard_map/ppermute | solution.py:20
  29.7 1.9 copy-start.6
  31.6 2.5 copy-start.4
  34.3 3.6 copy-start.5
  42.6 17.4 %copy-start.3 = (bf16[1024,2048]{1,0:T(8,128)(2,1)S(1)}, bf16[1024,2048]{1,0:T(8,128)(2,1)}, u32[]{:S(2)}) copy-start(bf16[1024,2048]{1,0:T(8,128)(2,1)} %param.15) | copy-start | bytes 12582916
  64.2 1.9 copy-start
  64.2 1.9 copy-start.8
  68.1 187.0 %all-gather.6.cloned.1.call-start = ((), (), s32[]{:S(2)}) async-start(), calls=%async_computation.3 | async-start | bytes 17825792 | tf_op jit(solution)/shard_map/all_gather | solution.py:100
  68.8 316.5 %all-gather.8.cloned.1.call-start = ((), (), s32[]{:S(2)}) async-start(), calls=%async_computation.4 | async-start | bytes 17825792 | tf_op jit(solution)/shard_map/all_gather | solution.py:101
  69.6 392.2 %reduce-scatter.2.cloned.1.call-start = ((), (), s32[]{:S(2)}) async-start(), calls=%async_computation.5 | async-start | bytes 6291456 | tf_op jit(solution)/shard_map/reduce_scatter | solution.py:120
  461.8 4.0 copy-start.1
  461.8 4.7 copy-start.2
  465.7 2.0 copy-start.9
Sparse Core Ops, SparseCore 0:
  68.2 58.2 all-gather.3
  128.6 126.4 all-gather.5
  257.3 128.0 all-gather.7
  409.2 52.5 reduce-scatter.1
where the time goes:
time: 478 us
  waiting for transfers between devices  347 us (73%)
  matrix products  56.9 us (12%)
  other arithmetic  21.8 us (5%)
  blocking collectives  17.2 us (4%)
  between operations  13.4 us (3%)
  starting transfers between devices  10.9 us (2%)
  local copies, waits for them, and re-layouts  10.6 us (2%)
    all_gather x1, waiting for transfers between devices, per_device(): up_whole = lax.all_gather(up_weight, 'sp', axis=0, tiled=True)  129 us
    all_gather x1, waiting for transfers between devices, per_device(): down_whole = lax.all_gather(down_weight, 'sp', axis=1, tiled=True)  107 us
    all_gather x1, waiting for transfers between devices, per_device(): lax.all_gather(first_stream, 'tp', axis=0, tiled=True)  56.9 us
    reduce_scatter x1, waiting for transfers between devices, per_device(): lax.psum_scatter(jnp.dot(active, down_whole, preferred_element_type=jnp.f...  52.7 us
    dot_general x1, matrix products, per_device(): jnp.dot(active, down_whole, preferred_element_type=jnp.float32)  23.7 us
    dot_general x1, matrix products, per_device(): jnp.dot(lax.all_gather(first_stream, 'tp', axis=0, tiled=True), up_whole,...  22.9 us
    all_to_all x1, blocking collectives, per_device(): lax.all_to_all(by_peer, 'tp', split_axis=0, concat_axis=2, tiled=True)[0]  17.2 us
  transfers between devices with their start and end apart: 8, of which 4 were waited for; matrix products, arithmetic and copies ran while one was open for 7% of the time, Pallas kernels for 0%

commit v1 on v0

--- a/solution.py
+++ b/solution.py
@@ -98,7 +98,7 @@
     second_gain,
 ):
     up_whole = lax.all_gather(up_weight, "sp", axis=0, tiled=True)
-    down_whole = lax.all_gather(down_weight, "sp", axis=1, tiled=True)
+    down_whole = jnp.concatenate(lax.all_gather(down_weight, "sp"), axis=1)
     attended = attend(queries, keyvals, head_sink_logit, doc_ids)
     tp_count = lax.axis_size("tp")
     own_rows = attended.shape[0] // tp_count

time: 478 us -> 439 us (0.918)
  waiting for transfers between devices: 347 us -> 286 us
  local copies, waits for them, and re-layouts: 10.6 us -> 32.3 us
    all_gather x1, waiting for transfers between devices: 107 us -> 68 us  [per_device(): down_whole = jnp.concatenate(lax.all_gather(down_weight, 'sp'), axis=1)]
    all_gather x1, waiting for transfers between devices: 56.9 us -> 35.3 us  [per_device(): lax.all_gather(first_stream, 'tp', axis=0, tiled=True)]
    reshape x0 -> x1, local copies, waits for them, and re-layouts: none -> 21.2 us  [per_device(): down_whole = jnp.concatenate(lax.all_gather(down_weight, 'sp'), axis=1)]
  transfers between devices with their start and end apart: 8 -> 8, of which waited for: 4 -> 4; matrix products, arithmetic and copies ran while one was open for 7% -> 13% of each run, Pallas kernels for 0% -> 0%
where the time goes in v1:
time: 439 us; the launch traced here: 438 us
  waiting for transfers between devices  286 us (65%)
  matrix products  54.7 us (12%)
  local copies, waits for them, and re-layouts  32.3 us (7%)
  other arithmetic  23.8 us (5%)
  blocking collectives  17.2 us (4%)
  between operations  13.4 us (3%)
  starting transfers between devices  10.9 us (2%)
    all_gather x1, waiting for transfers between devices, per_device(): up_whole = lax.all_gather(up_weight, 'sp', axis=0, tiled=True)  129 us
    all_gather x1, waiting for transfers between devices, per_device(): down_whole = jnp.concatenate(lax.all_gather(down_weight, 'sp'), axis=1)  68 us
    reduce_scatter x1, waiting for transfers between devices, per_device(): lax.psum_scatter(jnp.dot(active, down_whole, preferred_element_type=jnp.f...  52.7 us
    all_gather x1, waiting for transfers between devices, per_device(): lax.all_gather(first_stream, 'tp', axis=0, tiled=True)  35.3 us
    dot_general x1, matrix products, per_device(): jnp.dot(lax.all_gather(first_stream, 'tp', axis=0, tiled=True), up_whole,...  23 us
    dot_general x1, matrix products, per_device(): jnp.dot(active, down_whole, preferred_element_type=jnp.float32)  21.4 us
    reshape x1, local copies, waits for them, and re-layouts, per_device(): down_whole = jnp.concatenate(lax.all_gather(down_weight, 'sp'), axis=1)  21.2 us
    all_to_all x1, blocking collectives, per_device(): lax.all_to_all(by_peer, 'tp', split_axis=0, concat_axis=2, tiled=True)[0]  17.2 us
  transfers between devices with their start and end apart: 8, of which 4 were waited for; matrix products, arithmetic and copies ran while one was open for 13% of the time, Pallas kernels for 0%

profile of v1, /device:TPU:0, one launch (start us, length us, event | category | flops | bytes accessed | tf_op | source)
XLA Modules:
  0.0 438.3 jit_solution(6287170292320835710)
XLA Ops:
  6.5 0.7 all-gather.9.cloned.1.call-update
  7.3 0.7 convert_element_type.34
  8.0 2.4 collective-permute-start.2
  10.4 1.3 collective-permute-start.3
  11.7 1.4 copy.40
  13.1 0.8 fusion.18
  13.8 5.8 %collective-permute-start = (bf16[128,4,128]{2,0,1:T(8,128)(2,1)}, bf16[128,4,128]{2,0,1:T(8,128)(2,1)}, u32[]{:S(2)}, u32[]{:S(2)}) collective-permute-start(bf16[128,4,128]{2,0,1:T(8,128)(2,1)} %get-tuple-element.7), channel_id=1, source_target_pairs={{0,2},{2,4},{4,6},{6,8},{8,10},{10,12},{12,14},{14,16},{16,18},{18... | collective-permute-start | bytes 393224 | tf_op jit(solution)/shard_map/ppermute | solution.py:17
  19.6 1.3 collective-permute-start.1
  21.5 0.7 convert_bitcast_fusion
  23.0 1.3 copy.46
  24.3 2.1 reshape.176
  27.1 3.1 fusion.9
  30.2 1.3 pad_maximum_fusion.2
  32.8 1.8 pad_maximum_fusion
  34.7 2.5 fusion.1
  37.4 3.4 fusion
  40.9 3.6 fusion.11
  44.5 0.7 copy.51
  45.9 17.2 %all_to_all.15 = bf16[2,512,512]{1,2,0:T(8,128)(2,1)S(1)} all-to-all(bf16[2,512,512]{1,2,0:T(8,128)(2,1)S(1)} %copy.52), channel_id=1, replica_groups=mesh['sp'=16,'tp'=2] {'tp'}, dimensions={0} | all-to-all | bytes 2097152 | tf_op jit(solution)/shard_map/all_to_all | solution.py:107
  63.0 4.2 fusion.20
  67.8 1.5 copy-done
  69.3 1.9 multiply_convert_fusion.2
  72.1 68.0 %all-gather.9.cloned.1.call-done = bf16[65536,128]{1,0:T(8,128)(2,1)} async-done(((bf16[4096,128]{1,0:T(8,128)(2,1)}), bf16[65536,128]{1,0:T(8,128)(2,1)}) %all-gather.9.cloned.1.call-update) | async-done | bytes 16777232 | tf_op jit(solution)/shard_map/all_gather | solution.py:101
  140.0 21.2 %copy.53 = bf16[4096,16,128]{0,2,1:T(8,128)(2,1)} copy(bf16[4096,16,128]{2,0,1:T(8,128)(2,1)} %bitcast.78) | data formatting | bytes 33554432 | tf_op jit(solution)/shard_map/reshape | solution.py:101
  161.2 35.3 %all-gather.5.cloned.1.call-done = bf16[1024,2048]{1,0:T(8,128)(2,1)} async-done(((bf16[512,2048]{1,0:T(8,128)(2,1)}), bf16[1024,2048]{1,0:T(8,128)(2,1)}) %all-gather.5.cloned.1.call-update) | async-done | bytes 4194320 | tf_op jit(solution)/shard_map/all_gather | solution.py:115
  196.5 128.6 %all-gather.7.cloned.1.call-done = bf16[2048,4096]{1,0:T(8,128)(2,1)} async-done(((bf16[128,4096]{1,0:T(8,128)(2,1)}), bf16[2048,4096]{1,0:T(8,128)(2,1)}) %all-gather.7.cloned.1.call-update) | async-done | bytes 16777232 | tf_op jit(solution)/shard_map/all_gather | solution.py:100
  325.1 23.0 %fusion.44 = bf16[1024,4096]{1,0:T(8,128)(2,1)} fusion(bf16[2048,4096]{1,0:T(8,128)(2,1)} %all-gather.7.cloned.1.call-done, bf16[1024,2048]{1,0:T(8,128)(2,1)} %all-gather.5.cloned.1.call-done), kind=kOutput, calls=%bitcast_fusion.1.clone.1 | convolution fusion | flops 17192452096 | bytes 29360128 | tf_op jit(solution)/shard_map/dot_general | solution.py:114
  348.2 21.4 %convolution_convert_fusion = bf16[1024,2048]{1,0:T(8,128)(2,1)} fusion(bf16[4096,2048]{0,1:T(8,128)(2,1)S(1)} %bitcast.79, bf16[1024,4096]{1,0:T(8,128)(2,1)} %fusion.44), kind=kOutput, calls=%fused_computation.15 | convolution fusion | flops 17181966336 | bytes 29360128 | tf_op jit(solution)/shard_map/dot_general | solution.py:121
  369.5 52.7 %reduce-scatter.2.cloned.1.call-done = bf16[512,2048]{1,0:T(8,128)(2,1)} async-done(((bf16[1024,2048]{1,0:T(8,128)(2,1)}), bf16[512,2048]{1,0:T(8,128)(2,1)}) %reduce-scatter.2.cloned.1.call-update) | async-done | bytes 2097168 | tf_op jit(solution)/shard_map/reduce_scatter | solution.py:120
  422.2 3.9 fusion.4
  426.9 1.2 multiply_reduce_fusion
  428.2 3.5 multiply_convert_fusion.1
  (57 shorter events, 6.4 us)
Async XLA Ops:
  6.5 16.4 %copy-start.5 = (bf16[1024,4,128]{2,1,0:T(4,128)(2,1)S(1)}, bf16[1024,4,128]{2,1,0:T(4,128)(2,1)}, u32[]{:S(2)}) copy-start(bf16[1024,4,128]{2,1,0:T(4,128)(2,1)} %param.11) | copy-start | bytes 3145732
  6.5 17.8 %copy-start.9 = (bf16[1024,512]{1,0:T(8,128)(2,1)S(1)}, bf16[1024,512]{1,0:T(8,128)(2,1)}, u32[]{:S(2)}) copy-start(bf16[1024,512]{1,0:T(8,128)(2,1)} %param.10) | copy-start | bytes 3145732
  6.5 133.5 %all-gather.9.cloned.1.call-start = ((), (), s32[]{:S(2)}) async-start(), calls=%async_computation.5 | async-start | bytes 17825792 | tf_op jit(solution)/shard_map/all_gather | solution.py:101
  7.3 19.1 %copy-start.13 = (f32[8]{0:T(128)S(1)}, f32[8]{0:T(128)}, u32[]{:S(2)}) copy-start(f32[8]{0:T(128)} %param.12) | copy-start | bytes 100
  7.3 189.2 %all-gather.5.cloned.1.call-start = ((), (), s32[]{:S(2)}) async-start(), calls=%async_computation.2 | async-start | bytes 6291456 | tf_op jit(solution)/shard_map/all_gather | solution.py:115
  8.0 19.0 %collective-permute-start.2 = (bf16[128]{0:T(256)(128)(2,1)S(1)}, bf16[128]{0:T(256)(128)(2,1)S(1)}, u32[]{:S(2)}, u32[]{:S(2)}) collective-permute-start(bf16[128]{0:T(256)(128)(2,1)S(1)} %get-tuple-element.11), channel_id=1, source_target_pairs={{0,2},{2,4},{4,6},{6,8},{8,10},{10,12},{12,14},{14,16},{16,18},{18... | collective-permute-start | bytes 776 | tf_op jit(solution)/shard_map/ppermute | solution.py:17
  10.4 16.6 %collective-permute-start.3 = (bf16[128]{0:T(256)(128)(2,1)S(1)}, bf16[128]{0:T(256)(128)(2,1)S(1)}, u32[]{:S(2)}, u32[]{:S(2)}) collective-permute-start(bf16[128]{0:T(256)(128)(2,1)S(1)} %get-tuple-element.12), channel_id=1, source_target_pairs={{2,0},{4,2},{6,4},{8,6},{10,8},{12,10},{14,12},{16,14},{18,16},{20... | collective-permute-start | bytes 776 | tf_op jit(solution)/shard_map/ppermute | solution.py:20
  13.8 16.4 %collective-permute-start = (bf16[128,4,128]{2,0,1:T(8,128)(2,1)}, bf16[128,4,128]{2,0,1:T(8,128)(2,1)}, u32[]{:S(2)}, u32[]{:S(2)}) collective-permute-start(bf16[128,4,128]{2,0,1:T(8,128)(2,1)} %get-tuple-element.7), channel_id=1, source_target_pairs={{0,2},{2,4},{4,6},{6,8},{8,10},{10,12},{12,14},{14,16},{16,18},{18... | collective-permute-start | bytes 393224 | tf_op jit(solution)/shard_map/ppermute | solution.py:17
  19.6 10.6 %collective-permute-start.1 = (bf16[128,4,128]{2,0,1:T(8,128)(2,1)}, bf16[128,4,128]{2,0,1:T(8,128)(2,1)}, u32[]{:S(2)}, u32[]{:S(2)}) collective-permute-start(bf16[128,4,128]{2,0,1:T(8,128)(2,1)} %get-tuple-element.8), channel_id=1, source_target_pairs={{2,0},{4,2},{6,4},{8,6},{10,8},{12,10},{14,12},{16,14},{18,16},{20... | collective-permute-start | bytes 393224 | tf_op jit(solution)/shard_map/ppermute | solution.py:20
  32.8 1.9 copy-start.8
  34.7 2.5 copy-start.6
  34.7 2.6 copy-start.11
  37.4 3.6 copy-start.7
  45.7 17.4 %copy-start.4 = (bf16[1024,2048]{1,0:T(8,128)(2,1)S(1)}, bf16[1024,2048]{1,0:T(8,128)(2,1)}, u32[]{:S(2)}) copy-start(bf16[1024,2048]{1,0:T(8,128)(2,1)} %param.15) | copy-start | bytes 12582916
  67.3 2.0 copy-start
  67.3 2.0 copy-start.10
  71.3 253.9 %all-gather.7.cloned.1.call-start = ((), (), s32[]{:S(2)}) async-start(), calls=%async_computation.3 | async-start | bytes 17825792 | tf_op jit(solution)/shard_map/all_gather | solution.py:100
  72.0 350.2 %reduce-scatter.2.cloned.1.call-start = ((), (), s32[]{:S(2)}) async-start(), calls=%async_computation.4 | async-start | bytes 6291456 | tf_op jit(solution)/shard_map/reduce_scatter | solution.py:120
  325.1 23.0 %copy-start.3 = (bf16[4096,16,128]{0,2,1:T(8,128)(2,1)S(1)}, bf16[4096,16,128]{0,2,1:T(8,128)(2,1)}, u32[]{:S(2)}) copy-start(bf16[4096,16,128]{0,2,1:T(8,128)(2,1)} %copy.53) | copy-start | bytes 50331652
  422.2 4.0 copy-start.1
  422.2 4.7 %copy-start.2 = (bf16[512,2048]{1,0:T(8,128)(2,1)S(1)}, bf16[512,2048]{1,0:T(8,128)(2,1)}, u32[]{:S(2)}) copy-start(bf16[512,2048]{1,0:T(8,128)(2,1)} %reduce-scatter.2.cloned.1.call-done) | copy-start | bytes 6291460
  426.2 2.0 copy-start.12
Sparse Core Ops, SparseCore 0:
  9.5 130.4 all-gather.8
  141.6 54.8 all-gather.4
  198.7 126.4 all-gather.6
  369.7 52.5 reduce-scatter.1
